TPU v7x, 32 devices: a whole 2x2x4 slice. The times are simulated.
32 devices in a mesh: sp: 8 (over z, y), tp: 4 (over x, core).
Axes of the slice: x: 2, y: 2, z: 4, core: 2. Of those that a mesh axis runs over, the one named last changes fastest.
Arguments:
- query_proj: bfloat16 [2048, 2048], P('sp', 'tp'), may hold values from -240 to 240
- key_projection: bfloat16 [2048, 512], P('sp', 'tp'), may hold values from -6 to 6
- value_projection: bfloat16 [2048, 512], P('sp', 'tp'), may hold values from -6 to 6
- sink_logit: float32 [32], P('tp'), may hold values from 1 to 6
- residual: bfloat16 [2048, 2048], P('sp'), may hold values from -3 to 3
- w_out: bfloat16 [2048, 2048], P('tp'), may hold values from -1 to 1
- norm_gain: float32 [2048], replicated, may hold values from 0.1 to 1.9
- routes: int32 [2048, 2], P('sp'), may hold values from 0 to 7, all different within a row; in each aligned block of 256 rows (0 to 255, 256 to 511, ...) at most 128 rows name the same one
- route_weights: float32 [2048, 2], P('sp'), may hold values from 0.1 to 1
- w_gate: bfloat16 [8, 2048, 2560], P('sp', None, 'tp'), may hold values from -0.125 to 0.125
- w_up: bfloat16 [8, 2048, 2560], P('sp', None, 'tp'), may hold values from -0.125 to 0.125
- w_down: bfloat16 [8, 2560, 2048], P('sp', 'tp'), may hold values from -0.125 to 0.125
Outputs:
- layer_out: bfloat16 [2048, 2048], P('sp', 'tp')
Inputs may be any that keep to these rules, and one draw needn't show every extreme that they name: `routes`: within the rows of one index of sp (aligned blocks of 256 tokens), no expert is named more than 128 times, and in some block one expert is named exactly 128 times. The two experts of a token differ.
All inputs are finite; a program needn't handle non-finite values.
Results may differ from a plain program's by a relative error of at most 0.015.
Values may be sent and summed in bfloat16 or wider, within the bound.
A program may use at most 64 MiB of HBM per device.

v0:
```python
import jax
import jax.numpy as jnp
from jax import lax
from jax.sharding import PartitionSpec as P

HEAD_SIZE = 64
WINDOW = 128
GRID_W = 64
ROPE_BASE = 10000.0
NORM_EPS = 1e-06


def padded(cells, sides, width):
    for axis, dim in sides:
        count = lax.axis_size(axis)
        ends = count - 1
        head = lax.slice_in_dim(cells, 0, width, axis=dim)
        tail = lax.slice_in_dim(cells, cells.shape[dim] - width, cells.shape[dim], axis=dim)
        cells = jnp.concatenate(
            [
                lax.ppermute(tail, axis, [(i, (i + 1) % count) for i in range(ends)]),
                cells,
                lax.ppermute(head, axis, [((i + 1) % count, i) for i in range(ends)]),
            ],
            axis=dim,
        )
    return cells


def rotate_pair(values_half, angles):
    first_half, second = jnp.split(values_half, 2, axis=-1)
    cosine = jnp.cos(angles)[:, None, :]
    sine_part = jnp.sin(angles)[:, None, :]
    return jnp.concatenate(
        [first_half * cosine - second * sine_part, second * cosine + first_half * sine_part],
        axis=-1,
    )


def axial_rotation(heads_in, token_positions):
    half_dim = HEAD_SIZE // 2
    inverse = ROPE_BASE ** (-jnp.arange(0, half_dim, 2, dtype=jnp.float32) / half_dim)
    row_angles = (token_positions // GRID_W).astype(jnp.float32)[:, None] * inverse
    col_angles = (token_positions % GRID_W).astype(jnp.float32)[:, None] * inverse
    as_float = heads_in.astype(jnp.float32)
    return jnp.concatenate(
        [
            rotate_pair(as_float[..., :half_dim], row_angles),
            rotate_pair(as_float[..., half_dim:], col_angles),
        ],
        axis=-1,
    )


def attend_block(query_rows, key_rows, value_rows, sink_logit, query_pos, key_pos, total_rows):
    kv_heads = key_rows.shape[1]
    groups = query_rows.shape[1] // kv_heads
    grouped = query_rows.reshape(query_rows.shape[0], kv_heads, groups, HEAD_SIZE)
    scores = jnp.einsum(
        "qkgd,jkd->kgqj", grouped, key_rows, preferred_element_type=jnp.float32
    ) * HEAD_SIZE ** (-0.5)
    in_window = (
        (jnp.abs(key_pos[None, :] - query_pos[:, None]) <= WINDOW)
        & (key_pos[None, :] >= 0)
        & (key_pos[None, :] < total_rows)
    )
    scores = jnp.where(in_window[None, None], scores, -jnp.inf)
    sink_col = sink_logit.reshape(kv_heads, groups, 1, 1)
    largest = jnp.maximum(jnp.max(scores, axis=-1, keepdims=True), sink_col)
    exp_scores = jnp.exp(scores - largest)
    denominator = jnp.sum(exp_scores, axis=-1, keepdims=True) + jnp.exp(sink_col - largest)
    weights_bf = (exp_scores / denominator).astype(jnp.bfloat16)
    mixed_heads = jnp.einsum(
        "kgqj,jkd->qkgd", weights_bf, value_rows, preferred_element_type=jnp.float32
    )
    return mixed_heads.astype(jnp.bfloat16).reshape(query_rows.shape[0], -1)


def local(
    query_proj,
    key_projection,
    value_projection,
    sink_logit,
    residual,
    w_out,
    norm_gain,
    routes,
    route_weights,
    w_gate,
    w_up,
    w_down,
):
    tok_rows = query_proj.shape[0]
    seq_devices = lax.axis_size("sp")
    total_rows = tok_rows * seq_devices
    offset = lax.axis_index("sp") * tok_rows
    kv_width = key_projection.shape[1]
    joined = jnp.concatenate([key_projection, value_projection], axis=1)
    widened = padded(joined, (("sp", 0),), WINDOW)
    query_pos = offset + jnp.arange(tok_rows, dtype=jnp.int32)
    key_pos = offset - WINDOW + jnp.arange(tok_rows + 2 * WINDOW, dtype=jnp.int32)
    rot_q = axial_rotation(query_proj.reshape(tok_rows, -1, HEAD_SIZE), query_pos).astype(
        jnp.bfloat16
    )
    rotated_keys = axial_rotation(
        widened[:, :kv_width].reshape(-1, kv_width // HEAD_SIZE, HEAD_SIZE), key_pos
    ).astype(jnp.bfloat16)
    value_head_rows = widened[:, kv_width:].reshape(-1, kv_width // HEAD_SIZE, HEAD_SIZE)
    attended = attend_block(
        rot_q, rotated_keys, value_head_rows, sink_logit, query_pos, key_pos, total_rows
    )
    partial_value = jnp.dot(attended, w_out, preferred_element_type=jnp.float32)
    width = partial_value.shape[1]
    col_blocks = lax.axis_size("tp")
    col_width = width // col_blocks
    col_start = lax.axis_index("tp") * col_width
    summed = lax.psum(partial_value.astype(jnp.bfloat16), "tp").astype(jnp.float32)
    stream = (residual.astype(jnp.float32) + summed).astype(jnp.bfloat16)
    as_float = stream.astype(jnp.float32)
    normed = (
        as_float
        * lax.rsqrt(jnp.mean(as_float * as_float, axis=-1, keepdims=True) + NORM_EPS)
        * norm_gain
    ).astype(jnp.bfloat16)
    stream_cols = lax.dynamic_slice_in_dim(stream, col_start, col_width, 1)
    top_count = routes.shape[1]
    experts = w_gate.shape[0] * seq_devices
    capacity = 2 * top_count * tok_rows // experts
    flat_routes = routes.reshape(-1)
    onehot = (flat_routes[:, None] == jnp.arange(experts, dtype=jnp.int32)[None, :]).astype(
        jnp.int32
    )
    slot_number = jnp.sum(jnp.cumsum(onehot, axis=0) * onehot, axis=1) - 1
    destination = flat_routes * capacity + slot_number
    buffer = (
        jnp.zeros((experts * capacity, width), jnp.bfloat16)
        .at[destination]
        .set(jnp.repeat(normed, top_count, axis=0))
        .reshape(experts, capacity, width)
    )
    quarter = capacity // col_blocks
    own_slots = lax.dynamic_slice_in_dim(buffer, lax.axis_index("tp") * quarter, quarter, 1)
    arrived = lax.all_to_all(own_slots, "sp", split_axis=0, concat_axis=0, tiled=True)
    joined_slots = lax.all_gather(arrived, "tp", axis=1, tiled=True)
    sources, slot_count, _ = joined_slots.shape
    expert_rows = joined_slots.reshape(-1, width)
    gate_part = jnp.dot(expert_rows, w_gate[0], preferred_element_type=jnp.float32)
    up_part = jnp.dot(expert_rows, w_up[0], preferred_element_type=jnp.float32)
    hidden = (jax.nn.silu(gate_part) * up_part).astype(jnp.bfloat16)
    partial_rows = jnp.dot(hidden, w_down[0], preferred_element_type=jnp.float32)
    col_sums = lax.psum_scatter(
        partial_rows.astype(jnp.bfloat16), "tp", scatter_dimension=1, tiled=True
    )
    returned = lax.all_to_all(
        col_sums.reshape(sources, slot_count, col_width),
        "sp",
        split_axis=0,
        concat_axis=0,
        tiled=True,
    )
    picked = (
        returned.reshape(-1, col_width)[destination]
        .astype(jnp.float32)
        .reshape(tok_rows, top_count, col_width)
    )
    mixture = jnp.sum(picked * route_weights[:, :, None], axis=1)
    return (stream_cols.astype(jnp.float32) + mixture).astype(jnp.bfloat16)


def solution(mesh):
    return jax.shard_map(
        local,
        mesh=mesh,
        in_specs=(
            P("sp", "tp"),
            P("sp", "tp"),
            P("sp", "tp"),
            P("tp"),
            P("sp", None),
            P("tp", None),
            P(),
            P("sp", None),
            P("sp", None),
            P("sp", None, "tp"),
            P("sp", None, "tp"),
            P("sp", "tp", None),
        ),
        out_specs=P("sp", "tp"),
        check_vma=False,
    )
```

profile of v0, /device:TPU:0, one launch (start us, length us, event | category | flops | bytes accessed | tf_op | source)
XLA Modules:
  0.0 277.2 jit_solution(1034085529072347477)
XLA Ops:
  6.5 1.0 constant_dynamic-update-slice_fusion.1
  7.5 0.9 constant_dynamic-update-slice_fusion
  8.4 0.6 fusion.50
  9.1 5.5 %collective-permute-start = (bf16[128,256]{1,0:T(8,128)(2,1)}, bf16[128,256]{1,0:T(8,128)(2,1)}, u32[]{:S(2)}, u32[]{:S(2)}) collective-permute-start(bf16[128,256]{1,0:T(8,128)(2,1)} %get-tuple-element.21), channel_id=1, source_target_pairs={{0,4},{4,8},{8,12},{12,16},{16,20},{20,24},{24,28},{1,5},{5,9},{9,... | collective-permute-start | bytes 196616 | tf_op jit(solution)/shard_map/ppermute | solution.py:21
  14.6 1.3 collective-permute-start.1
  15.9 0.5 multiply_power_fusion
  16.4 0.6 fusion.43
  16.9 0.6 fusion.44
  17.5 0.6 fusion.39
  18.1 0.6 iota_add_fusion
  18.7 0.8 copy.26
  19.5 0.1 eq.33
  19.7 0.7 eq.29
  20.4 1.3 broadcast_multiply_fusion
  21.7 1.1 copy.23
  22.8 1.3 max.18
  24.1 1.5 multiply_cosine_fusion.1
  25.6 0.9 multiply_cosine_fusion.3
  26.5 1.1 reduce-window.6
  27.6 0.9 fusion.19
  28.6 0.8 subtract_convert_fusion.1
  29.3 0.2 slice_reduce_fusion
  29.6 0.6 slice.35
  30.2 0.8 copy.25
  31.0 0.7 mul.319
  31.7 0.0 collective-permute-done.1
  31.7 0.9 pad_maximum_fusion
  32.7 0.1 copy.22
  32.8 0.8 subtract_convert_fusion.3
  33.7 1.7 fusion.1
  35.4 0.1 broadcast_maximum_fusion
  35.5 1.8 copy-done.2
  37.3 0.9 fusion
  38.2 0.1 exponential_add_fusion
  38.3 0.1 copy.21
  38.4 0.0 copy-start.3
  38.4 3.5 %fusion.15 = bf16[2,64,4,256]{3,1,2,0:T(8,128)(2,1)S(1)} fusion(bf16[512,2,64,1]{0,2,3,1:T(8,128)(2,1)S(1)} %bitcast.68, f32[2,512,256,4]{2,1,3,0:T(8,128)} %copy-done.2, f32[2,4,256]{2,1,0:T(4,128)S(1)} %exponential_add_fusion, f32[2,4,256]{2,1,0:T(4,128)S(1)} %broadcast_maximum_fusion, pred[256,512]{0,1:T(8,128)(4,1)S(1)} %fusion.19), kind=kOutput, calls=%fused_computation.24 | convolution fusion | flops 139591680 | bytes 4734976 | tf_op jit(solution)/shard_map/kgqj,jkd->qkgd/dot_general | solution.py:73
  42.0 1.8 convolution_convert_fusion.1
  43.8 0.0 all-reduce.2.cloned.1.call-update
  43.8 0.2 all-gather.2.cloned.1.call-start
  44.1 0.1 fusion.34
  44.2 38.5 %all-reduce.2.cloned.1.call-done = bf16[256,2048]{1,0:T(8,128)(2,1)} async-done(((bf16[256,2048]{1,0:T(8,128)(2,1)}), bf16[256,2048]{1,0:T(8,128)(2,1)}) %all-reduce.2.cloned.1.call-update) | async-done | bytes 1048592 | tf_op jit(solution)/shard_map/psum | solution.py:117
  82.7 2.0 fusion.7
  84.7 1.0 copy-done.1
  85.7 0.3 fusion.9
  86.0 2.6 broadcast_in_dim.15
  88.6 4.1 %reshape.478 = bf16[512,2048]{1,0:T(8,128)(2,1)} reshape(bf16[256,2,2048]{2,1,0:T(2,128)(2,1)} %broadcast_in_dim.15) | data formatting | bytes 4194304 | tf_op jit(solution)/shard_map/reshape | solution.py:138
  92.7 7.2 %scatter_custom_fusion = bf16[1024,2048]{1,0:T(8,128)(2,1)} fusion(s32[512]{0:T(512)S(1)} %bitcast.73, bf16[512,2048]{1,0:T(8,128)(2,1)} %reshape.478, bf16[]{:T(256)} %constant.97.clone.1), kind=kCustom, calls=%fused_computation.20 | custom fusion | bytes 4194816 | tf_op jit(solution)/shard_map/scatter | solution.py:138
  99.9 1.3 constant_dynamic-slice_fusion
  101.2 30.7 %all_to_all.10 = bf16[8,32,2048]{2,1,0:T(8,128)(2,1)} all-to-all(bf16[8,32,2048]{2,1,0:T(8,128)(2,1)S(1)} %constant_dynamic-slice_fusion), channel_id=1, replica_groups=mesh['sp'=8,'tp'=4] {'sp'}, dimensions={0} | all-to-all | bytes 2097152 | tf_op jit(solution)/shard_map/all_to_all | solution.py:143
  131.9 0.0 all-gather.2.cloned.1.call-update
  131.9 0.3 reduce-scatter.2.cloned.1.call-start
  132.2 33.2 %all-gather.2.cloned.1.call-done = bf16[8,128,2048]{2,1,0:T(8,128)(2,1)} async-done(((bf16[8,32,2048]{2,1,0:T(8,128)(2,1)}), bf16[8,128,2048]{2,1,0:T(8,128)(2,1)}) %all-gather.2.cloned.1.call-update) | async-done | bytes 4194320 | tf_op jit(solution)/shard_map/all_gather | solution.py:144
  165.4 8.0 %fusion.3 = f32[1024,640]{1,0:T(8,128)} fusion(bf16[1024,2048]{1,0:T(8,128)(2,1)} %bitcast.76, bf16[1,2048,640]{2,1,0:T(8,128)(2,1)} %param.22), kind=kOutput, calls=%fused_computation.11 | convolution fusion | flops 2684354560 | bytes 9437184 | tf_op jit(solution)/shard_map/dot_general | solution.py:148
  173.4 12.1 %convolution_convert_fusion = bf16[1024,2048]{1,0:T(8,128)(2,1)} fusion(bf16[1,640,2048]{2,1,0:T(8,128)(2,1)S(1)} %copy-done, f32[1024,640]{1,0:T(8,128)} %fusion.3, bf16[1024,2048]{1,0:T(8,128)(2,1)} %bitcast.77, bf16[1,2048,640]{2,1,0:T(8,128)(2,1)} %param.21), kind=kOutput, calls=%fused_computation.5 | convolution fusion | flops 5374738432 | bytes 16252928 | tf_op jit(solution)/shard_map/dot_general | solution.py:150
  185.5 0.0 reduce-scatter.2.cloned.1.call-update
  185.5 44.6 %reduce-scatter.2.cloned.1.call-done = bf16[1024,512]{1,0:T(8,128)(2,1)} async-done(((bf16[1024,2048]{1,0:T(8,128)(2,1)}), bf16[1024,512]{1,0:T(8,128)(2,1)}) %reduce-scatter.2.cloned.1.call-update) | async-done | bytes 1048592 | tf_op jit(solution)/shard_map/reduce_scatter | solution.py:151
  230.1 5.5 %all-to-all-start.1 = ((bf16[8,128,512]{2,1,0:T(8,128)(2,1)}), bf16[8,128,512]{2,1,0:T(8,128)(2,1)}, u32[]{:S(2)}, u32[]{:S(2)}) async-start(bf16[8,128,512]{2,1,0:T(8,128)(2,1)} %bitcast.65), calls=%async_computation.2 | async-start | bytes 2097152 | tf_op jit(solution)/shard_map/all_to_all | solution.py:154
  235.6 0.1 copy.28
  235.8 25.6 %all-to-all-done.1 = bf16[8,128,512]{2,1,0:T(8,128)(2,1)} async-done(((bf16[8,128,512]{2,1,0:T(8,128)(2,1)}), bf16[8,128,512]{2,1,0:T(8,128)(2,1)}, u32[]{:S(2)}, u32[]{:S(2)}) %all-to-all-start.1) | async-done | bytes 1048608 | tf_op jit(solution)/shard_map/all_to_all | solution.py:154
  261.4 3.3 %gather_fusion = bf16[512,512]{1,0:T(8,128)(2,1)S(1)} fusion(bf16[1024,512]{1,0:T(8,128)(2,1)} %bitcast.25, s32[1024]{0:T(1024)S(1)} %pad_clamp_fusion), kind=kCustom, calls=%fused_computation | custom fusion | bytes 1050624 | tf_op jit(solution)/shard_map/gather | solution.py:162
  264.7 1.6 reshape.465
  266.3 2.6 multiply_reduce_fusion
  268.9 1.7 add_convert_fusion.1
  (28 shorter events, 0.2 us)
Async XLA Ops:
  6.5 166.9 %copy-start = (bf16[1,640,2048]{2,1,0:T(8,128)(2,1)S(1)}, bf16[1,640,2048]{2,1,0:T(8,128)(2,1)}, u32[]{:S(2)}) copy-start(bf16[1,640,2048]{2,1,0:T(8,128)(2,1)} %param.23) | copy-start | bytes 7864324
  6.5 76.1 %all-reduce.2.cloned.1.call-start = ((), (), s32[]{:S(2)}) async-start(), calls=%async_computation.3 | async-start | bytes 2097152 | tf_op jit(solution)/shard_map/psum | solution.py:117
  9.1 22.7 %collective-permute-start = (bf16[128,256]{1,0:T(8,128)(2,1)}, bf16[128,256]{1,0:T(8,128)(2,1)}, u32[]{:S(2)}, u32[]{:S(2)}) collective-permute-start(bf16[128,256]{1,0:T(8,128)(2,1)} %get-tuple-element.21), channel_id=1, source_target_pairs={{0,4},{4,8},{8,12},{12,16},{16,20},{20,24},{24,28},{1,5},{5,9},{9,... | collective-permute-start | bytes 196616 | tf_op jit(solution)/shard_map/ppermute | solution.py:21
  14.6 17.2 %collective-permute-start.1 = (bf16[128,256]{1,0:T(8,128)(2,1)}, bf16[128,256]{1,0:T(8,128)(2,1)}, u32[]{:S(2)}, u32[]{:S(2)}) collective-permute-start(bf16[128,256]{1,0:T(8,128)(2,1)} %get-tuple-element.22), channel_id=1, source_target_pairs={{4,0},{8,4},{12,8},{16,12},{20,16},{24,20},{28,24},{5,1},{9,5},{13... | collective-permute-start | bytes 196616 | tf_op jit(solution)/shard_map/ppermute | solution.py:23
  33.6 1.8 copy-start.8
  35.4 1.9 copy-start.2
  38.4 3.6 %copy-start.3 = (bf16[512,2048]{1,0:T(8,128)(2,1)S(1)}, bf16[512,2048]{1,0:T(8,128)(2,1)}, u32[]{:S(2)}) copy-start(bf16[512,2048]{1,0:T(8,128)(2,1)} %param.17) | copy-start | bytes 6291460
  42.0 2.0 copy-start.6
  42.0 2.1 copy-start.7
  42.0 2.1 copy-start.5
  43.8 41.9 %copy-start.4 = (f32[2048]{0:T(1024)S(1)}, f32[2048]{0:T(1024)}, u32[]{:S(2)}) copy-start(f32[2048]{0:T(1024)} %param.18) | copy-start | bytes 24580
  43.8 121.6 %all-gather.2.cloned.1.call-start = ((), (), s32[]{:S(2)}) async-start(), calls=%async_computation.4 | async-start | bytes 5242880 | tf_op jit(solution)/shard_map/all_gather | solution.py:144
  84.7 1.0 copy-start.1
  131.9 98.2 %reduce-scatter.2.cloned.1.call-start = ((), (), s32[]{:S(2)}) async-start(), calls=%async_computation.5 | async-start | bytes 5242880 | tf_op jit(solution)/shard_map/reduce_scatter | solution.py:151
  185.5 50.1 %copy-start.9 = (f32[256,2]{0,1:T(2,128)S(1)}, f32[256,2]{0,1:T(2,128)}, u32[]{:S(2)}) copy-start(f32[256,2]{0,1:T(2,128)} %param.20) | copy-start | bytes 6148
  230.1 31.3 %all-to-all-start.1 = ((bf16[8,128,512]{2,1,0:T(8,128)(2,1)}), bf16[8,128,512]{2,1,0:T(8,128)(2,1)}, u32[]{:S(2)}, u32[]{:S(2)}) async-start(bf16[8,128,512]{2,1,0:T(8,128)(2,1)} %bitcast.65), calls=%async_computation.2 | async-start | bytes 2097152 | tf_op jit(solution)/shard_map/all_to_all | solution.py:154
Sparse Core Ops, SparseCore 0:
  43.9 38.7 all-reduce.1
  132.0 33.3 all-gather.1
  185.6 44.4 reduce-scatter.1
where the time goes:
time: 278 us; the launch traced here: 277 us
  waiting for transfers between devices  142 us (51%)
  local copies, waits for them, and re-layouts  32.3 us (12%)
  blocking collectives  30.7 us (11%)
  matrix products  27.1 us (10%)
  other arithmetic  19 us (7%)
  between operations  13.4 us (5%)
  starting transfers between devices  12.8 us (5%)
    reduce_scatter x1, waiting for transfers between devices, local(): lax.psum_scatter(partial_rows.astype(jnp.bfloat16), 'tp', scatter_dimensi...  44.6 us
    psum x1, waiting for transfers between devices, local(): lax.psum(partial_value.astype(jnp.bfloat16), 'tp').astype(jnp.float32)  38.5 us
    all_gather x1, waiting for transfers between devices, local(): joined_slots = lax.all_gather(arrived, 'tp', axis=1, tiled=True)  33.2 us
    all_to_all x1, blocking collectives, local(): lax.all_to_all(own_slots, 'sp', split_axis=0, concat_axis=0, tiled=True)  30.7 us
    all_to_all x1, waiting for transfers between devices, local(): lax.all_to_all(col_sums.reshape(sources, slot_count, col_width), 'sp', sp...  25.6 us
    dot_general x1, matrix products, local(): jnp.dot(hidden, w_down[0], preferred_element_type=jnp.float32)  12.1 us
    dot_general x1, matrix products, local(): up_part = jnp.dot(expert_rows, w_up[0], preferred_element_type=jnp.float32)  8 us
    scatter x1, local copies, waits for them, and re-layouts, local(): buffer = jnp.zeros((experts * capacity, width), jnp.bfloat16).at[destinat...  7.21 us
  transfers between devices with their start and end apart: 6, of which 4 were waited for; matrix products, arithmetic and copies ran while one was open for 6% of the time, Pallas kernels for 0%

commit v1 on v0

--- a/solution.py
+++ b/solution.py
@@ -114,7 +114,9 @@
     col_blocks = lax.axis_size("tp")
     col_width = width // col_blocks
     col_start = lax.axis_index("tp") * col_width
-    summed = lax.psum(partial_value.astype(jnp.bfloat16), "tp").astype(jnp.float32)
+    summed = jnp.sum(lax.all_gather(partial_value.astype(jnp.bfloat16), "tp"), axis=0).astype(
+        jnp.float32
+    )
     stream = (residual.astype(jnp.float32) + summed).astype(jnp.bfloat16)
     as_float = stream.astype(jnp.float32)
     normed = (

time: 278 us -> 265 us (0.953)
  waiting for transfers between devices: 142 us -> 137 us
  local copies, waits for them, and re-layouts: 32.3 us -> 28.1 us
  other arithmetic: 19 us -> 15 us
    psum x1 -> x0, waiting for transfers between devices: 38.5 us -> none  [local(): lax.psum(partial_value.astype(jnp.bfloat16), 'tp').astype(jnp.float32)]
    all_gather x0 -> x1, waiting for transfers between devices: none -> 33.2 us  [local(): lax.all_gather(partial_value.astype(jnp.bfloat16), 'tp')]
    reduce_sum x0 -> x1, other arithmetic: none -> 4.25 us  [local(): jnp.sum(lax.all_gather(partial_value.astype(jnp.bfloat16), 'tp'), axis=0)]
    unnamed x24 -> x18, local copies, waits for them, and re-layouts: 5.85 us -> 5.18 us
  transfers between devices with their start and end apart: 6 -> 6, of which waited for: 4 -> 5; matrix products, arithmetic and copies ran while one was open for 6% -> 2% of each run, Pallas kernels for 0% -> 0%
where the time goes in v1:
time: 265 us
  waiting for transfers between devices  137 us (52%)
  blocking collectives  31.5 us (12%)
  local copies, waits for them, and re-layouts  28.1 us (11%)
  matrix products  27.1 us (10%)
  other arithmetic  15 us (6%)
  between operations  13.4 us (5%)
  starting transfers between devices  12.2 us (5%)
    reduce_scatter x1, waiting for transfers between devices, local(): lax.psum_scatter(partial_rows.astype(jnp.bfloat16), 'tp', scatter_dimensi...  44.6 us
    all_gather x1, waiting for transfers between devices, local(): lax.all_gather(partial_value.astype(jnp.bfloat16), 'tp')  33.2 us
    all_gather x1, waiting for transfers between devices, local(): joined_slots = lax.all_gather(arrived, 'tp', axis=1, tiled=True)  32.5 us
    all_to_all x1, blocking collectives, local(): lax.all_to_all(own_slots, 'sp', split_axis=0, concat_axis=0, tiled=True)  31.5 us
    all_to_all x1, waiting for transfers between devices, local(): lax.all_to_all(col_sums.reshape(sources, slot_count, col_width), 'sp', sp...  25.6 us
    dot_general x1, matrix products, local(): jnp.dot(hidden, w_down[0], preferred_element_type=jnp.float32)  12.1 us
    dot_general x1, matrix products, local(): up_part = jnp.dot(expert_rows, w_up[0], preferred_element_type=jnp.float32)  8 us
    scatter x1, local copies, waits for them, and re-layouts, local(): buffer = jnp.zeros((experts * capacity, width), jnp.bfloat16).at[destinat...  7.21 us
  transfers between devices with their start and end apart: 6, of which 5 were waited for; matrix products, arithmetic and copies ran while one was open for 2% of the time, Pallas kernels for 0%

profile of v1, /device:TPU:0, one launch (start us, length us, event | category | flops | bytes accessed | tf_op | source)
XLA Modules:
  0.0 264.5 jit_solution(3567403814526736775)
XLA Ops:
  6.5 0.0 copy-start
  6.5 0.0 all-gather.6.cloned.1.call-start
  6.5 1.0 constant_dynamic-update-slice_fusion.1
  7.5 0.9 constant_dynamic-update-slice_fusion
  8.4 4.9 %collective-permute-start = (bf16[128,256]{1,0:T(8,128)(2,1)S(1)}, bf16[128,256]{1,0:T(8,128)(2,1)S(1)}, u32[]{:S(2)}, u32[]{:S(2)}) collective-permute-start(bf16[128,256]{1,0:T(8,128)(2,1)S(1)} %get-tuple-element.21), channel_id=1, source_target_pairs={{0,4},{4,8},{8,12},{12,16},{16,20},{20,24},{24,28},{1,5},{5,9},{9,... | collective-permute-start | bytes 196616 | tf_op jit(solution)/shard_map/ppermute | solution.py:21
  13.3 1.3 collective-permute-start.1
  14.7 1.1 copy.23
  15.9 0.3 multiply_cosine_fusion.1
  16.2 0.2 multiply_cosine_fusion.3
  16.4 0.7 subtract_convert_fusion.1
  17.1 0.3 fusion.19
  17.4 0.7 max.18
  18.2 0.0 collective-permute-done
  18.2 1.3 collective-permute-done.1
  19.6 0.1 copy.22
  19.7 1.7 fusion.1
  21.5 0.0 copy-start.2
  21.5 0.1 broadcast_maximum_fusion
  21.6 1.8 copy-done.2
  23.4 0.9 fusion
  24.3 0.1 exponential_add_fusion
  24.4 0.1 copy.21
  24.5 0.0 copy-start.3
  24.5 3.5 %fusion.15 = bf16[2,64,4,256]{3,1,2,0:T(8,128)(2,1)S(1)} fusion(bf16[512,2,64,1]{0,2,3,1:T(8,128)(2,1)S(1)} %bitcast.70, f32[2,512,256,4]{2,1,3,0:T(8,128)} %copy-done.2, f32[2,4,256]{2,1,0:T(4,128)S(1)} %exponential_add_fusion, f32[2,4,256]{2,1,0:T(4,128)S(1)} %broadcast_maximum_fusion, pred[256,512]{0,1:T(8,128)(4,1)S(1)} %fusion.19), kind=kOutput, calls=%fused_computation.24 | convolution fusion | flops 139591680 | bytes 4734976 | tf_op jit(solution)/shard_map/kgqj,jkd->qkgd/dot_general | solution.py:73
  28.1 0.0 copy-start.5
  28.1 0.0 copy-done.3
  28.1 1.7 convolution_convert_fusion.1
  29.8 0.0 all-gather.6.cloned.1.call-update
  29.8 0.2 all-gather.4.cloned.1.call-start
  30.1 0.0 copy-done.5
  30.1 0.1 copy.26
  30.2 0.1 eq.33
  30.4 0.1 eq.29
  30.5 1.1 reduce-window.6
  31.7 0.2 slice_reduce_fusion
  31.9 0.1 copy.25
  32.1 0.1 mul.319
  32.2 0.1 fusion.34
  32.3 33.2 %all-gather.6.cloned.1.call-done = bf16[1024,2048]{1,0:T(8,128)(2,1)} async-done(((bf16[256,2048]{1,0:T(8,128)(2,1)}), bf16[1024,2048]{1,0:T(8,128)(2,1)}) %all-gather.6.cloned.1.call-update) | async-done | bytes 4194320 | tf_op jit(solution)/shard_map/all_gather | solution.py:117
  65.6 4.3 %reduce_sum.49 = bf16[256,2048]{1,0:T(8,128)(2,1)} reduce(bf16[4,256,2048]{2,1,0:T(8,128)(2,1)} %bitcast.65, bf16[]{:T(256)} %constant.96.clone.1), dimensions={0}, to_apply=%region_2.3 | reduce | flops 1572864 | bytes 5242882 | tf_op jit(solution)/shard_map/reduce_sum | solution.py:117
  69.8 2.1 fusion.7
  71.9 1.0 copy-done.1
  72.9 0.0 copy-done.4
  72.9 0.3 fusion.9
  73.2 2.6 broadcast_in_dim.15
  75.8 4.1 %reshape.478 = bf16[512,2048]{1,0:T(8,128)(2,1)} reshape(bf16[256,2,2048]{2,1,0:T(2,128)(2,1)} %broadcast_in_dim.15) | data formatting | bytes 4194304 | tf_op jit(solution)/shard_map/reshape | solution.py:140
  79.9 7.2 %scatter_custom_fusion = bf16[1024,2048]{1,0:T(8,128)(2,1)} fusion(s32[512]{0:T(512)S(1)} %bitcast.75, bf16[512,2048]{1,0:T(8,128)(2,1)} %reshape.478, bf16[]{:T(256)} %constant.96.clone.1), kind=kCustom, calls=%fused_computation.20 | custom fusion | bytes 4194816 | tf_op jit(solution)/shard_map/scatter | solution.py:140
  87.1 1.3 constant_dynamic-slice_fusion
  88.4 31.5 %all_to_all.10 = bf16[8,32,2048]{2,1,0:T(8,128)(2,1)} all-to-all(bf16[8,32,2048]{2,1,0:T(8,128)(2,1)S(1)} %constant_dynamic-slice_fusion), channel_id=1, replica_groups=mesh['sp'=8,'tp'=4] {'sp'}, dimensions={0} | all-to-all | bytes 2097152 | tf_op jit(solution)/shard_map/all_to_all | solution.py:145
  120.0 0.0 all-gather.4.cloned.1.call-update
  120.0 0.3 reduce-scatter.2.cloned.1.call-start
  120.3 32.5 %all-gather.4.cloned.1.call-done = bf16[8,128,2048]{2,1,0:T(8,128)(2,1)} async-done(((bf16[8,32,2048]{2,1,0:T(8,128)(2,1)}), bf16[8,128,2048]{2,1,0:T(8,128)(2,1)}) %all-gather.4.cloned.1.call-update) | async-done | bytes 4194320 | tf_op jit(solution)/shard_map/all_gather | solution.py:146
  152.7 8.0 %fusion.3 = f32[1024,640]{1,0:T(8,128)} fusion(bf16[1024,2048]{1,0:T(8,128)(2,1)} %bitcast.78, bf16[1,2048,640]{2,1,0:T(8,128)(2,1)} %param.22), kind=kOutput, calls=%fused_computation.11 | convolution fusion | flops 2684354560 | bytes 9437184 | tf_op jit(solution)/shard_map/dot_general | solution.py:150
  160.7 0.0 copy-done
  160.7 12.1 %convolution_convert_fusion = bf16[1024,2048]{1,0:T(8,128)(2,1)} fusion(bf16[1,640,2048]{2,1,0:T(8,128)(2,1)S(1)} %copy-done, f32[1024,640]{1,0:T(8,128)} %fusion.3, bf16[1024,2048]{1,0:T(8,128)(2,1)} %bitcast.79, bf16[1,2048,640]{2,1,0:T(8,128)(2,1)} %param.21), kind=kOutput, calls=%fused_computation.5 | convolution fusion | flops 5374738432 | bytes 16252928 | tf_op jit(solution)/shard_map/dot_general | solution.py:152
  172.8 0.0 reduce-scatter.2.cloned.1.call-update
  172.8 44.6 %reduce-scatter.2.cloned.1.call-done = bf16[1024,512]{1,0:T(8,128)(2,1)} async-done(((bf16[1024,2048]{1,0:T(8,128)(2,1)}), bf16[1024,512]{1,0:T(8,128)(2,1)}) %reduce-scatter.2.cloned.1.call-update) | async-done | bytes 1048592 | tf_op jit(solution)/shard_map/reduce_scatter | solution.py:153
  217.4 5.5 %all-to-all-start.1 = ((bf16[8,128,512]{2,1,0:T(8,128)(2,1)}), bf16[8,128,512]{2,1,0:T(8,128)(2,1)}, u32[]{:S(2)}, u32[]{:S(2)}) async-start(bf16[8,128,512]{2,1,0:T(8,128)(2,1)} %bitcast.67), calls=%async_computation.2 | async-start | bytes 2097152 | tf_op jit(solution)/shard_map/all_to_all | solution.py:156
  222.9 0.1 copy.28
  223.1 25.6 %all-to-all-done.1 = bf16[8,128,512]{2,1,0:T(8,128)(2,1)} async-done(((bf16[8,128,512]{2,1,0:T(8,128)(2,1)}), bf16[8,128,512]{2,1,0:T(8,128)(2,1)}, u32[]{:S(2)}, u32[]{:S(2)}) %all-to-all-start.1) | async-done | bytes 1048608 | tf_op jit(solution)/shard_map/all_to_all | solution.py:156
  248.7 3.3 %gather_fusion = bf16[512,512]{1,0:T(8,128)(2,1)S(1)} fusion(bf16[1024,512]{1,0:T(8,128)(2,1)} %bitcast.26, s32[1024]{0:T(1024)S(1)} %pad_clamp_fusion), kind=kCustom, calls=%fused_computation | custom fusion | bytes 1050624 | tf_op jit(solution)/shard_map/gather | solution.py:164
  252.0 1.6 reshape.465
  253.7 2.6 multiply_reduce_fusion
  256.3 1.7 add_convert_fusion.1
  (23 shorter events, 0.3 us)
Async XLA Ops:
  6.5 154.2 %copy-start = (bf16[1,640,2048]{2,1,0:T(8,128)(2,1)S(1)}, bf16[1,640,2048]{2,1,0:T(8,128)(2,1)}, u32[]{:S(2)}) copy-start(bf16[1,640,2048]{2,1,0:T(8,128)(2,1)} %param.23) | copy-start | bytes 7864324
  6.5 59.0 %all-gather.6.cloned.1.call-start = ((), (), s32[]{:S(2)}) async-start(), calls=%async_computation.5 | async-start | bytes 5242880 | tf_op jit(solution)/shard_map/all_gather | solution.py:117
  8.4 9.7 %collective-permute-start = (bf16[128,256]{1,0:T(8,128)(2,1)S(1)}, bf16[128,256]{1,0:T(8,128)(2,1)S(1)}, u32[]{:S(2)}, u32[]{:S(2)}) collective-permute-start(bf16[128,256]{1,0:T(8,128)(2,1)S(1)} %get-tuple-element.21), channel_id=1, source_target_pairs={{0,4},{4,8},{8,12},{12,16},{16,20},{20,24},{24,28},{1,5},{5,9},{9,... | collective-permute-start | bytes 196616 | tf_op jit(solution)/shard_map/ppermute | solution.py:21
  13.3 6.2 %collective-permute-start.1 = (bf16[128,256]{1,0:T(8,128)(2,1)S(1)}, bf16[128,256]{1,0:T(8,128)(2,1)S(1)}, u32[]{:S(2)}, u32[]{:S(2)}) collective-permute-start(bf16[128,256]{1,0:T(8,128)(2,1)S(1)} %get-tuple-element.22), channel_id=1, source_target_pairs={{4,0},{8,4},{12,8},{16,12},{20,16},{24,20},{28,24},{5,1},{9,5},{13... | collective-permute-start | bytes 196616 | tf_op jit(solution)/shard_map/ppermute | solution.py:23
  21.5 1.9 copy-start.2
  24.5 3.6 %copy-start.3 = (bf16[512,2048]{1,0:T(8,128)(2,1)S(1)}, bf16[512,2048]{1,0:T(8,128)(2,1)}, u32[]{:S(2)}) copy-start(bf16[512,2048]{1,0:T(8,128)(2,1)} %param.17) | copy-start | bytes 6291460
  28.1 2.0 copy-start.5
  29.8 122.9 %all-gather.4.cloned.1.call-start = ((), (), s32[]{:S(2)}) async-start(), calls=%async_computation.3 | async-start | bytes 5242880 | tf_op jit(solution)/shard_map/all_gather | solution.py:146
  69.8 3.0 %copy-start.4 = (f32[2048]{0:T(1024)S(1)}, f32[2048]{0:T(1024)}, u32[]{:S(2)}) copy-start(f32[2048]{0:T(1024)} %param.18) | copy-start | bytes 24580
  71.9 1.0 copy-start.1
  120.0 97.4 %reduce-scatter.2.cloned.1.call-start = ((), (), s32[]{:S(2)}) async-start(), calls=%async_computation.4 | async-start | bytes 5242880 | tf_op jit(solution)/shard_map/reduce_scatter | solution.py:153
  172.8 50.1 %copy-start.6 = (f32[256,2]{0,1:T(2,128)S(1)}, f32[256,2]{0,1:T(2,128)}, u32[]{:S(2)}) copy-start(f32[256,2]{0,1:T(2,128)} %param.20) | copy-start | bytes 6148
  217.4 31.3 %all-to-all-start.1 = ((bf16[8,128,512]{2,1,0:T(8,128)(2,1)}), bf16[8,128,512]{2,1,0:T(8,128)(2,1)}, u32[]{:S(2)}, u32[]{:S(2)}) async-start(bf16[8,128,512]{2,1,0:T(8,128)(2,1)} %bitcast.67), calls=%async_computation.2 | async-start | bytes 2097152 | tf_op jit(solution)/shard_map/all_to_all | solution.py:156
Sparse Core Ops, SparseCore 0:
  29.9 35.5 all-gather.5
  120.1 32.5 all-gather.3
  173.0 44.4 reduce-scatter.1
